TPU v7x, 32 devices: a whole 2x2x4 slice. The times are simulated.
32 devices in a mesh: kv: 8 (over z, core), tp: 4 (over y, x).
Axes of the slice: x: 2, y: 2, z: 4, core: 2. Of those that a mesh axis runs over, the one named last changes fastest.
Arguments:
- tokens: bfloat16 [64, 4096], P(None, ('kv', 'tp')), may hold values from -3 to 3
- lengths: int32 [16], replicated, may hold values from 1 to 4, 32 in all
- states: float32 [16, 16, 128, 128], P('kv', 'tp'), may hold values from -3 to 3
- gain_pre: float32 [4096], P('kv'), may hold values from 0.1 to 1.9
- pre_gate: bfloat16 [4096, 11264], P('kv', 'tp'), may hold values from -0.09375 to 0.09375
- pre_up: bfloat16 [4096, 11264], P('kv', 'tp'), may hold values from -0.09375 to 0.09375
- pre_down: bfloat16 [11264, 4096], P('tp', 'kv'), may hold values from -1 to 1
- gain_mix: float32 [4096], P('kv'), may hold values from 0.1 to 1.9
- query_weight: bfloat16 [4096, 2048], P('kv', 'tp'), may hold values from -0.09375 to 0.09375
- forget_weight: bfloat16 [4096, 2048], P('kv', 'tp'), may hold values from -0.09375 to 0.09375
- input_weight: bfloat16 [4096, 2048], P('kv', 'tp'), may hold values from -0.09375 to 0.09375
- outgate_weight: bfloat16 [4096, 2048], P('kv', 'tp'), may hold values from -0.09375 to 0.09375
- forget_floor: float32 [2048], P('tp'), may hold values from 0 to 0.9
- head_gain: float32 [128], replicated, may hold values from 0.1 to 1.9
- mix_weight: bfloat16 [2048, 4096], P('tp', 'kv'), may hold values from -1 to 1
- gain_post: float32 [4096], P('kv'), may hold values from 0.1 to 1.9
- post_gate: bfloat16 [4096, 11264], P('kv', 'tp'), may hold values from -0.09375 to 0.09375
- post_up: bfloat16 [4096, 11264], P('kv', 'tp'), may hold values from -0.09375 to 0.09375
- post_down: bfloat16 [11264, 4096], P('tp', 'kv'), may hold values from -0.0546875 to 0.0546875
Outputs:
- out_tokens: bfloat16 [64, 4096], P(None, ('kv', 'tp'))
- new_states: float32 [16, 16, 128, 128], P('kv', 'tp')
Inputs may be any that keep to these rules, and one draw needn't show every extreme that they name: `lengths`: each of the 16 sequences has 1 to 4 new tokens, 32 in all, and at least one has exactly 4.
All inputs are finite; a program needn't handle non-finite values.
Results may differ from a plain program's by a relative error of at most 0.011.
Values may be sent and summed in bfloat16 or wider, within the bound.
A program may use at most 64 MiB of HBM per device.

v0:
```python
import jax
import jax.numpy as jnp
from jax import lax
from jax.sharding import PartitionSpec as P

D = 4096
DK = 128
W = 4


EPSILON = 1e-06


def gathered_norm(shard, gain_block):
    gathered = lax.all_gather(shard, "tp", axis=1, tiled=True)
    block_squares = jnp.sum(jnp.square(gathered.astype(jnp.float32)), axis=1)
    totals = lax.psum(block_squares, "kv")
    scale = lax.rsqrt(totals[:, None] / D + EPSILON)
    return (gathered.astype(jnp.float32) * scale * gain_block).astype(jnp.bfloat16)


def half_mixer(shard, gain_block, gate_weight, up_weight, down_weight):
    normed = gathered_norm(shard, gain_block)
    half_cols = gate_weight.shape[1]
    owned = lax.psum_scatter(
        jnp.concatenate(
            [
                jnp.dot(normed, gate_weight, preferred_element_type=jnp.float32),
                jnp.dot(normed, up_weight, preferred_element_type=jnp.float32),
            ],
            axis=1,
        ),
        "kv",
        scatter_dimension=0,
        tiled=True,
    )
    hidden = (jax.nn.silu(owned[:, :half_cols]) * owned[:, half_cols:]).astype(jnp.bfloat16)
    partial_out = jnp.dot(
        lax.all_gather(hidden, "kv", axis=0, tiled=True),
        down_weight,
        preferred_element_type=jnp.float32,
    )
    return lax.psum_scatter(partial_out, "tp", scatter_dimension=1, tiled=True)


def local(
    tokens,
    lengths,
    states,
    gain_pre,
    pre_gate,
    pre_up,
    pre_down,
    gain_mix,
    query_weight,
    forget_weight,
    input_weight,
    outgate_weight,
    forget_floor,
    head_gain,
    mix_weight,
    gain_post,
    post_gate,
    post_up,
    post_down,
):
    resid_one = (
        tokens.astype(jnp.float32) + 0.5 * half_mixer(tokens, gain_pre, pre_gate, pre_up, pre_down)
    ).astype(jnp.bfloat16)
    normed = gathered_norm(resid_one, gain_mix)
    head_cols = query_weight.shape[1]
    seq_local = states.shape[0]
    heads_local = states.shape[1]
    owned = lax.psum_scatter(
        jnp.concatenate(
            [
                jnp.dot(normed, query_weight, preferred_element_type=jnp.float32),
                jnp.dot(normed, forget_weight, preferred_element_type=jnp.float32),
                jnp.dot(normed, input_weight, preferred_element_type=jnp.float32),
                jnp.dot(normed, outgate_weight, preferred_element_type=jnp.float32),
            ],
            axis=1,
        ),
        "kv",
        scatter_dimension=0,
        tiled=True,
    )
    shape_four = (seq_local, W, heads_local, DK)
    queries = jax.nn.silu(owned[:, :head_cols]).reshape(shape_four)
    forget_raw = owned[:, head_cols : 2 * head_cols].reshape(shape_four)
    fresh_values = owned[:, 2 * head_cols : 3 * head_cols].reshape(shape_four)
    gating = owned[:, 3 * head_cols :].reshape(shape_four)
    local_lengths = lax.dynamic_slice_in_dim(lengths, lax.axis_index("kv") * seq_local, seq_local)
    live_mask = jnp.arange(W, dtype=jnp.int32)[None, :] < local_lengths[:, None]
    live_four = live_mask[:, :, None, None]
    floors = forget_floor.reshape(heads_local, DK)
    forgets = jnp.where(
        live_four, floors + (1.0 - floors) * jax.nn.sigmoid(forget_raw), jnp.float32(1.0)
    )
    write_rate = 1.0 - forgets
    carried = states
    readings = []
    for offset in range(W):
        carried = (
            forgets[:, offset, :, :, None] * carried
            + write_rate[:, offset, :, :, None] * fresh_values[:, offset, :, None, :]
        )
        readings.append(
            jnp.einsum(
                "bhk,bhkv->bhv", queries[:, offset], carried, precision=lax.Precision.HIGHEST
            )
        )
    read_out = jnp.stack(readings, axis=1)
    meansq = jnp.mean(read_out * read_out, axis=3, keepdims=True)
    head_out = (
        (
            read_out
            * lax.rsqrt(meansq + EPSILON)
            * head_gain
            * jax.nn.silu(gating)
            * live_four.astype(jnp.float32)
        )
        .astype(jnp.bfloat16)
        .reshape(seq_local * W, heads_local * DK)
    )
    mixed_part = jnp.dot(
        lax.all_gather(head_out, "kv", axis=0, tiled=True),
        mix_weight,
        preferred_element_type=jnp.float32,
    )
    mixed = lax.psum_scatter(mixed_part, "tp", scatter_dimension=1, tiled=True)
    resid_two = (resid_one.astype(jnp.float32) + mixed).astype(jnp.bfloat16)
    finished = resid_two.astype(jnp.float32) + 0.5 * half_mixer(
        resid_two, gain_post, post_gate, post_up, post_down
    )
    live_rows = (
        (jnp.arange(W, dtype=jnp.int32)[None, :] < lengths[:, None])
        .reshape(-1, 1)
        .astype(jnp.float32)
    )
    outcome = (finished * live_rows).astype(jnp.bfloat16)
    return (outcome, carried)


def solution(mesh):
    placed = (
        P(None, ("kv", "tp")),
        P(),
        P("kv", "tp", None, None),
        P("kv"),
        P("kv", "tp"),
        P("kv", "tp"),
        P("tp", "kv"),
        P("kv"),
        P("kv", "tp"),
        P("kv", "tp"),
        P("kv", "tp"),
        P("kv", "tp"),
        P("tp"),
        P(),
        P("tp", "kv"),
        P("kv"),
        P("kv", "tp"),
        P("kv", "tp"),
        P("tp", "kv"),
    )
    return jax.shard_map(
        local,
        mesh=mesh,
        in_specs=placed,
        out_specs=(P(None, ("kv", "tp")), P("kv", "tp", None, None)),
        check_vma=False,
    )
```

profile of v0, /device:TPU:0, one launch (start us, length us, event | category | flops | bytes accessed | tf_op | source)
XLA Modules:
  0.0 318.7 jit_solution(17917307360592700447)
XLA Ops:
  7.2 10.1 %all_gather.18 = bf16[64,512]{1,0:T(8,128)(2,1)S(1)} all-gather(bf16[64,128]{1,0:T(8,128)(2,1)} %param.19), channel_id=1, replica_groups=mesh['kv'=8,'tp'=4] {'tp'}, dimensions={1}, use_global_device_ids=true | all-gather | bytes 81920 | tf_op jit(solution)/shard_map/all_gather | solution.py:15
  17.3 0.1 fusion.8
  17.5 14.9 %psum.21 = f32[64]{0:T(128)S(1)} all-reduce(f32[64]{0:T(128)S(1)} %fusion.8), channel_id=1, replica_groups=mesh['kv'=8,'tp'=4] {'kv'}, use_global_device_ids=true, to_apply=%region_1.0 | all-reduce | flops 64 | bytes 512 | tf_op jit(solution)/shard_map/psum | solution.py:17
  32.4 1.5 fusion.26
  33.9 0.3 copy-done.1
  34.2 0.7 fusion.24
  34.8 1.2 pad_maximum_fusion
  36.1 31.3 %reduce-scatter.7.cloned.1.call-done = f32[8,5632]{1,0:T(8,128)} async-done(((f32[64,5632]{1,0:T(8,128)}), f32[8,5632]{1,0:T(8,128)}) %reduce-scatter.7.cloned.1.call-update) | async-done | bytes 180240 | tf_op jit(solution)/shard_map/reduce_scatter | solution.py:25
  67.4 1.0 fusion.19
  68.4 14.4 %all_gather.19 = bf16[64,2816]{1,0:T(8,128)(2,1)S(1)} all-gather(bf16[8,2816]{1,0:T(8,128)(2,1)S(1)} %fusion.19), channel_id=1, replica_groups=mesh['kv'=8,'tp'=4] {'kv'}, dimensions={0}, use_global_device_ids=true | all-gather | bytes 405504 | tf_op jit(solution)/shard_map/all_gather | solution.py:39
  82.7 3.1 fusion.45
  85.9 22.2 %reduce-scatter.9.cloned.1.call-done = f32[64,128]{1,0:T(8,128)} async-done(((f32[64,512]{1,0:T(8,128)}), f32[64,128]{1,0:T(8,128)}) %reduce-scatter.9.cloned.1.call-update) | async-done | bytes 32784 | tf_op jit(solution)/shard_map/reduce_scatter | solution.py:43
  108.1 0.8 add_convert_fusion.1
  108.8 8.1 %all_gather.20 = bf16[64,512]{1,0:T(8,128)(2,1)S(1)} all-gather(bf16[64,128]{1,0:T(8,128)(2,1)S(1)} %add_convert_fusion.1), channel_id=1, replica_groups=mesh['kv'=8,'tp'=4] {'tp'}, dimensions={1}, use_global_device_ids=true | all-gather | bytes 81920 | tf_op jit(solution)/shard_map/all_gather | solution.py:15
  117.0 0.1 fusion.11
  117.1 13.9 %psum.22 = f32[64]{0:T(128)S(1)} all-reduce(f32[64]{0:T(128)S(1)} %fusion.11), channel_id=1, replica_groups=mesh['kv'=8,'tp'=4] {'kv'}, use_global_device_ids=true, to_apply=%region_5.6 | all-reduce | flops 64 | bytes 512 | tf_op jit(solution)/shard_map/psum | solution.py:17
  131.0 1.3 fusion.42
  132.3 1.3 fusion.40
  133.6 1.3 fusion.38
  134.9 1.3 fusion.36
  136.2 0.8 pad_maximum_fusion.2
  137.3 28.2 %reduce-scatter.11.cloned.1.call-done = f32[8,2048]{1,0:T(8,128)} async-done(((f32[64,2048]{1,0:T(8,128)}), f32[8,2048]{1,0:T(8,128)}) %reduce-scatter.11.cloned.1.call-update) | async-done | bytes 65552 | tf_op jit(solution)/shard_map/reduce_scatter | solution.py:74
  165.6 0.8 fusion.33
  166.5 0.8 fusion
  167.3 1.1 fusion.17
  168.4 1.5 fusion.1
  169.9 1.3 multiply_add_fusion
  171.2 0.8 copy-done.4
  172.0 0.5 fusion.46
  172.5 0.1 multiply_reduce_fusion
  172.7 0.8 fusion.30
  173.5 14.0 %all_gather.21 = bf16[64,512]{1,0:T(8,128)(2,1)S(1)} all-gather(bf16[8,512]{1,0:T(8,128)(2,1)S(1)} %fusion.30), channel_id=1, replica_groups=mesh['kv'=8,'tp'=4] {'kv'}, dimensions={0}, use_global_device_ids=true | all-gather | bytes 73728 | tf_op jit(solution)/shard_map/all_gather | solution.py:127
  187.5 0.8 fusion.47
  188.4 22.4 %reduce-scatter.13.cloned.1.call-done = f32[64,128]{1,0:T(8,128)} async-done(((f32[64,512]{1,0:T(8,128)}), f32[64,128]{1,0:T(8,128)}) %reduce-scatter.13.cloned.1.call-update) | async-done | bytes 32784 | tf_op jit(solution)/shard_map/reduce_scatter | solution.py:131
  210.8 0.8 add_convert_fusion
  211.5 8.2 %all_gather.22 = bf16[64,512]{1,0:T(8,128)(2,1)S(1)} all-gather(bf16[64,128]{1,0:T(8,128)(2,1)S(1)} %add_convert_fusion), channel_id=1, replica_groups=mesh['kv'=8,'tp'=4] {'tp'}, dimensions={1}, use_global_device_ids=true | all-gather | bytes 81920 | tf_op jit(solution)/shard_map/all_gather | solution.py:15
  219.7 0.1 fusion.14
  219.8 13.9 %psum.23 = f32[64]{0:T(128)S(1)} all-reduce(f32[64]{0:T(128)S(1)} %fusion.14), channel_id=1, replica_groups=mesh['kv'=8,'tp'=4] {'kv'}, use_global_device_ids=true, to_apply=%region_10.11 | all-reduce | flops 64 | bytes 512 | tf_op jit(solution)/shard_map/psum | solution.py:17
  233.7 2.6 fusion.22
  236.4 0.7 fusion.20
  237.0 1.2 pad_maximum_fusion.1
  238.3 31.2 %reduce-scatter.15.cloned.1.call-done = f32[8,5632]{1,0:T(8,128)} async-done(((f32[64,5632]{1,0:T(8,128)}), f32[8,5632]{1,0:T(8,128)}) %reduce-scatter.15.cloned.1.call-update) | async-done | bytes 180240 | tf_op jit(solution)/shard_map/reduce_scatter | solution.py:25
  269.6 1.0 fusion.18
  270.5 14.4 %all_gather.23 = bf16[64,2816]{1,0:T(8,128)(2,1)S(1)} all-gather(bf16[8,2816]{1,0:T(8,128)(2,1)S(1)} %fusion.18), channel_id=1, replica_groups=mesh['kv'=8,'tp'=4] {'kv'}, dimensions={0}, use_global_device_ids=true | all-gather | bytes 405504 | tf_op jit(solution)/shard_map/all_gather | solution.py:39
  284.9 3.1 fusion.48
  288.1 0.1 reshape.130
  288.1 22.2 %reduce-scatter.17.cloned.1.call-done = f32[64,128]{1,0:T(8,128)} async-done(((f32[64,512]{1,0:T(8,128)}), f32[64,128]{1,0:T(8,128)}) %reduce-scatter.17.cloned.1.call-update) | async-done | bytes 32784 | tf_op jit(solution)/shard_map/reduce_scatter | solution.py:43
  310.4 1.4 multiply_convert_fusion
  (54 shorter events, 1.0 us)
Async XLA Ops:
  7.2 25.2 %copy-start = (bf16[512,2816]{1,0:T(8,128)(2,1)S(1)}, bf16[512,2816]{1,0:T(8,128)(2,1)}, u32[]{:S(2)}) copy-start(bf16[512,2816]{1,0:T(8,128)(2,1)} %param.23) | copy-start | bytes 8650756
  7.2 26.7 %copy-start.8 = (f32[512]{0:T(512)S(1)}, f32[512]{0:T(512)}, u32[]{:S(2)}) copy-start(f32[512]{0:T(512)} %param.22) | copy-start | bytes 6148
  7.2 60.2 %reduce-scatter.7.cloned.1.call-start = ((), (), s32[]{:S(2)}) async-start(), calls=%async_computation.6 | async-start | bytes 1622016 | tf_op jit(solution)/shard_map/reduce_scatter | solution.py:25
  32.3 1.8 copy-start.1
  36.1 72.0 %copy-start.6 = (bf16[64,128]{1,0:T(8,128)(2,1)S(1)}, bf16[64,128]{1,0:T(8,128)(2,1)}, u32[]{:S(2)}) copy-start(bf16[64,128]{1,0:T(8,128)(2,1)} %param.19) | copy-start | bytes 49156
  36.1 94.9 %copy-start.7 = (f32[512]{0:T(512)S(1)}, f32[512]{0:T(512)}, u32[]{:S(2)}) copy-start(f32[512]{0:T(512)} %param.26) | copy-start | bytes 6148
  36.1 72.0 %reduce-scatter.9.cloned.1.call-start = ((), (), s32[]{:S(2)}) async-start(), calls=%async_computation.7 | async-start | bytes 163840 | tf_op jit(solution)/shard_map/reduce_scatter | solution.py:43
  85.8 51.2 %copy-start.12 = (s32[16]{0:T(128)S(1)}, s32[16]{0:T(128)}, u32[]{:S(2)}) copy-start(s32[16]{0:T(128)} %param.20) | copy-start | bytes 196
  85.8 51.5 %copy-start.11 = (f32[128]{0:T(128)S(1)}, f32[128]{0:T(128)}, u32[]{:S(2)}) copy-start(f32[128]{0:T(128)} %param.32) | copy-start | bytes 1540
  85.8 51.5 %copy-start.10 = (f32[512]{0:T(512)S(1)}, f32[512]{0:T(512)}, u32[]{:S(2)}) copy-start(f32[512]{0:T(512)} %param.31) | copy-start | bytes 6148
  85.8 80.7 %copy-start.3 = (f32[2,4,128,128]{3,2,1,0:T(8,128)S(1)}, f32[2,4,128,128]{3,2,1,0:T(8,128)}, u32[]{:S(2)}) copy-start(f32[2,4,128,128]{3,2,1,0:T(8,128)} %param.21) | copy-start | bytes 1572868
  85.9 79.7 %reduce-scatter.11.cloned.1.call-start = ((), (), s32[]{:S(2)}) async-start(), calls=%async_computation.8 | async-start | bytes 589824 | tf_op jit(solution)/shard_map/reduce_scatter | solution.py:74
  137.0 73.8 %reduce-scatter.13.cloned.1.call-start = ((), (), s32[]{:S(2)}) async-start(), calls=%async_computation.9 | async-start | bytes 163840 | tf_op jit(solution)/shard_map/reduce_scatter | solution.py:131
  166.4 21.1 %copy-start.5 = (bf16[512,512]{1,0:T(8,128)(2,1)S(1)}, bf16[512,512]{1,0:T(8,128)(2,1)}, u32[]{:S(2)}) copy-start(bf16[512,512]{1,0:T(8,128)(2,1)} %param.33) | copy-start | bytes 1572868
  166.5 67.2 %copy-start.9 = (f32[512]{0:T(512)S(1)}, f32[512]{0:T(512)}, u32[]{:S(2)}) copy-start(f32[512]{0:T(512)} %param.34) | copy-start | bytes 6148
  171.2 0.8 copy-start.4
  188.3 81.2 %reduce-scatter.15.cloned.1.call-start = ((), (), s32[]{:S(2)}) async-start(), calls=%async_computation.10 | async-start | bytes 1622016 | tf_op jit(solution)/shard_map/reduce_scatter | solution.py:25
  233.7 2.7 copy-start.2
  238.3 72.1 %reduce-scatter.17.cloned.1.call-start = ((), (), s32[]{:S(2)}) async-start(), calls=%async_computation.11 | async-start | bytes 163840 | tf_op jit(solution)/shard_map/reduce_scatter | solution.py:43
Sparse Core Ops, SparseCore 0:
  36.2 31.1 reduce-scatter.6
  86.0 22.0 reduce-scatter.8
  137.1 28.3 reduce-scatter.10
  188.4 22.2 reduce-scatter.12
  238.4 31.1 reduce-scatter.14
  288.1 22.2 reduce-scatter.16
where the time goes:
time: 320 us; the launch traced here: 319 us
  waiting for transfers between devices  158 us (49%)
  blocking collectives  112 us (35%)
  matrix products  21.5 us (7%)
  between operations  14.3 us (4%)
  other arithmetic  11.7 us (4%)
    reduce_scatter x2, waiting for transfers between devices, half_mixer(): lax.psum_scatter(jnp.concatenate([jnp.dot(normed, gate_weight, preferred_...  62.5 us
    reduce_scatter x2, waiting for transfers between devices, half_mixer(): return lax.psum_scatter(partial_out, 'tp', scatter_dimension=1, tiled=True)  44.4 us
    psum x3, blocking collectives, gathered_norm(): totals = lax.psum(block_squares, 'kv')  42.6 us
    all_gather x2, blocking collectives, half_mixer(): lax.all_gather(hidden, 'kv', axis=0, tiled=True)  28.7 us
    reduce_scatter x1, waiting for transfers between devices, local(): lax.psum_scatter(jnp.concatenate([jnp.dot(normed, query_weight, preferred...  28.2 us
    all_gather x3, blocking collectives, gathered_norm(): gathered = lax.all_gather(shard, 'tp', axis=1, tiled=True)  26.4 us
    reduce_scatter x1, waiting for transfers between devices, local(): mixed = lax.psum_scatter(mixed_part, 'tp', scatter_dimension=1, tiled=True)  22.4 us
    all_gather x1, blocking collectives, local(): lax.all_gather(head_out, 'kv', axis=0, tiled=True)  14 us
  transfers between devices with their start and end apart: 6, of which 6 were waited for; matrix products, arithmetic and copies ran while one was open for 0% of the time, Pallas kernels for 0%

commit v1 on v0

v1 whole, which is shorter than its diff:
```python
import functools

import jax
import jax.numpy as jnp
from jax import lax
from jax.experimental import pallas as pl
from jax.experimental.pallas import tpu as pltpu
from jax.sharding import PartitionSpec as P

D = 4096
DK = 128
W = 4
EPSILON = 1e-06
MESH = pl.DeviceIdType.MESH
F32 = jnp.float32
BF16 = jnp.bfloat16
CORES = 2


def silu(v):
    return v / (1.0 + jnp.exp(-v))


def sigmoid(v):
    return 1.0 / (1.0 + jnp.exp(-v))


def kernel(cfg, *refs):
    NK, NT, C, FL, HL, ROWS, aligned, nch = cfg
    NZ = NK // CORES
    RL = ROWS // NK
    FC = FL // nch
    it = iter(refs)
    (tokens, lengths, states_h, g_pre, pg_h, pu_h, pd_h, g_mix, q_h, f_h, i_h, o_h, floor, head_gain, mw_h,
     g_post, sg_h, su_h, sd_h) = [next(it) for _ in range(19)]
    out, ns_h = next(it), next(it)
    (x0, x1, x2, wpg, wpu, wpd, wq, wmw, wsg, wsu, wsd, st, tok_s, tok_r, w_sem, st_sem) = [
        next(it) for _ in range(16)]
    sq_bufs = [[next(it) for _ in range(4)] for _ in range(3)]
    ffn_bufs = [[next(it) for _ in range(14)] for _ in range(2)]
    mix_bufs = [next(it) for _ in range(9)]
    hg_bufs = [next(it) for _ in range(3)]
    ro = next(it)
    ar_bufs = [[next(it) for _ in range(3)] for _ in range(3)]
    fin = [next(it) for _ in range(2)]

    k = lax.axis_index("kv")
    t = lax.axis_index("tp")
    z = k // CORES
    c = k % CORES
    oc = 1 - c
    partner = (z * CORES + oc, t)
    pending = []

    def send(src, dst, ssem, rsem, dev):
        cp = pltpu.make_async_remote_copy(
            src_ref=src, dst_ref=dst, send_sem=ssem, recv_sem=rsem, device_id=dev, device_id_type=MESH)
        cp.start()
        pending.append(cp)

    def arrived(dst, ssem, rsem):
        pltpu.make_async_remote_copy(
            src_ref=dst, dst_ref=dst, send_sem=ssem, recv_sem=rsem, device_id=partner,
            device_id_type=MESH).wait_recv()

    def load(src, dst, sem):
        cp = pltpu.make_async_copy(src, dst, sem)
        cp.start()
        return cp

    def cols(j):
        return pl.ds(j * FC, FC)

    sem_n = iter(range(64))
    pre_loads = []
    for j in range(nch):
        pre_loads.append([
            load(pg_h.at[:, cols(j)], wpg.at[:, cols(j)], w_sem.at[next(sem_n)]),
            load(pu_h.at[:, cols(j)], wpu.at[:, cols(j)], w_sem.at[next(sem_n)])])

    barrier = pltpu.get_barrier_semaphore()
    for d in range(1, NK):
        pl.semaphore_signal(barrier, inc=1, device_id=((k + d) % NK, t), device_id_type=MESH)
    for d in range(1, NT):
        pl.semaphore_signal(barrier, inc=1, device_id=(k, (t + d) % NT), device_id_type=MESH)
    pl.semaphore_wait(barrier, NK - 1 + NT - 1)

    if aligned:
        w_tok = tokens.shape[1]
        mine = pl.ds(pl.multiple_of(t * w_tok, w_tok), w_tok)
        for d in range(1, NT):
            send(tokens, x0.at[:, mine], tok_s.at[d - 1], tok_r.at[d - 1], (k, (t + d) % NT))
        x0[:, mine] = tokens[...]
        for d in range(1, NT):
            src = (t - d + NT) % NT
            arrived(x0.at[:, pl.ds(pl.multiple_of(src * w_tok, w_tok), w_tok)], tok_s.at[d - 1], tok_r.at[d - 1])
    else:
        x0[...] = tokens[...]

    def squares(x32, bufs):
        s_buf, r_buf, ss, rs = bufs
        ssq = jnp.sum(x32 * x32, axis=1, keepdims=True)
        s_buf[...] = jnp.broadcast_to(ssq, (ROWS, 128)).reshape(NK, RL, 128)
        for d in range(1, NK):
            peer = (k + d) % NK
            send(s_buf.at[peer], r_buf.at[d - 1], ss.at[d - 1], rs.at[d - 1], (peer, t))

    def row_scale(bufs):
        s_buf, r_buf, ss, rs = bufs
        total = s_buf[k]
        for d in range(1, NK):
            arrived(r_buf.at[d - 1], ss.at[d - 1], rs.at[d - 1])
            total = total + r_buf[d - 1]
        return lax.rsqrt(total[:, :1] / D + EPSILON)

    z_order = sorted(range(1, NZ), key=lambda d: -min(d, NZ - d))

    def reduce_start(j, a, s1, r1, e_s, e_r):
        s1[j] = a[j, :, :, oc].astype(BF16)
        send(s1.at[j], r1.at[j], e_s.at[j], e_r.at[j], partner)

    def reduce_middle(j, a, r1, s2, r2, e_s, e_r, z_s, z_r):
        arrived(r1.at[j], e_s.at[j], e_r.at[j])
        for d in z_order:
            zp = (z + d) % NZ
            s2[j, d - 1] = (a[j, :, zp, c] + r1[j, :, zp].astype(F32)).astype(BF16)
            send(s2.at[j, d - 1], r2.at[j, d - 1], z_s.at[j, d - 1], z_r.at[j, d - 1], (zp * CORES + c, t))

    def reduce_end(j, a, r1, r2, z_s, z_r):
        total = a[j, :, z, c] + r1[j, :, z].astype(F32)
        for d in range(1, NZ):
            arrived(r2.at[j, d - 1], z_s.at[j, d - 1], z_r.at[j, d - 1])
            total = total + r2[j, d - 1].astype(F32)
        return total

    def block(x32, gain, wg, wu, wd, gu_loads, d_loads, after, sq, bufs):
        a, s1, r1, s2, r2, hid, e_s, e_r, z_s, z_r, h_s, h_r, p_s, p_r = bufs
        squares(x32, sq)
        y = (x32 * gain[...]).astype(BF16)
        for j in range(nch):
            for cp in gu_loads[j]:
                cp.wait()
            if j == nch - 1:
                after()
            for g, w in enumerate((wg, wu)):
                prod = jnp.dot(y, w[:, cols(j)], preferred_element_type=F32)
                a[j, g] = prod.reshape(NZ, CORES, RL, FC)
            reduce_start(j, a, s1, r1, e_s, e_r)
        for j in range(nch):
            reduce_middle(j, a, r1, s2, r2, e_s, e_r, z_s, z_r)
        scale = row_scale(sq)
        for j in range(nch):
            total = reduce_end(j, a, r1, r2, z_s, z_r)
            hid[j, z, c] = (silu(total[0] * scale) * (total[1] * scale)).astype(BF16)
            own = hid.at[j, z, c]
            for d in z_order:
                send(own, own, h_s.at[j, d - 1], h_r.at[j, d - 1], (((z + d) % NZ) * CORES + c, t))
            send(own, own, p_s.at[j, 0], p_r.at[j, 0], partner)
        for j in range(nch):
            for d in reversed(z_order):
                src = hid.at[j, (z - d + NZ) % NZ, c]
                arrived(src, h_s.at[j, d - 1], h_r.at[j, d - 1])
                send(src, src, p_s.at[j, d], p_r.at[j, d], partner)
        part = None
        for j in range(nch):
            d_loads[j].wait()
            for d in range(NZ):
                arrived(hid.at[j, (z - d + NZ) % NZ, oc], p_s.at[j, d], p_r.at[j, d])
            h = hid[j].astype(F32).reshape(ROWS, FC).astype(BF16)
            term = jnp.dot(h, wd[pl.ds(j * FC, FC), :], preferred_element_type=F32)
            part = term if part is None else part + term
        return part

    def sum_tp(part, bufs):
        buf, ss, rs = bufs
        buf[t] = part.astype(BF16)
        for d in range(1, NT):
            send(buf.at[t], buf.at[t], ss.at[d - 1], rs.at[d - 1], (k, (t + d) % NT))
        for d in range(1, NT):
            arrived(buf.at[(t - d + NT) % NT], ss.at[d - 1], rs.at[d - 1])
        total = buf[0].astype(F32)
        for s in range(1, NT):
            total = total + buf[s].astype(F32)
        return total

    later = {}

    def start_later():
        later["pd"] = [load(pd_h.at[pl.ds(j * FC, FC)], wpd.at[pl.ds(j * FC, FC)], w_sem.at[next(sem_n)])
                       for j in range(nch)]
        later["q"] = [load(h, wq.at[n], w_sem.at[next(sem_n)]) for n, h in enumerate((q_h, f_h, i_h, o_h))]
        later["st"] = load(states_h, st, st_sem.at[0])
        later["mw"] = load(mw_h, wmw, w_sem.at[next(sem_n)])
        later["sgu"] = [[load(sg_h.at[:, cols(j)], wsg.at[:, cols(j)], w_sem.at[next(sem_n)]),
                         load(su_h.at[:, cols(j)], wsu.at[:, cols(j)], w_sem.at[next(sem_n)])]
                        for j in range(nch)]
        later["sd"] = [load(sd_h.at[pl.ds(j * FC, FC)], wsd.at[pl.ds(j * FC, FC)], w_sem.at[next(sem_n)])
                       for j in range(nch)]

    class Lazy:
        def __getitem__(self, j):
            return later["pd"][j]

    part = block(x0[...].astype(F32), g_pre, wpg, wpu, wpd, pre_loads, Lazy(), start_later, sq_bufs[0], ffn_bufs[0])
    total = sum_tp(part, ar_bufs[0])
    x1[...] = (x0[...].astype(F32) + 0.5 * total).astype(BF16)

    x32 = x1[...].astype(F32)
    a, s1, r1, s2, r2, e_s, e_r, z_s, z_r = mix_bufs
    squares(x32, sq_bufs[1])
    y = (x32 * g_mix[...]).astype(BF16)
    for g in range(4):
        later["q"][g].wait()
        a[0, g] = jnp.dot(y, wq[g], preferred_element_type=F32).reshape(NZ, CORES, RL, HL)
    reduce_start(0, a, s1, r1, e_s, e_r)
    reduce_middle(0, a, r1, s2, r2, e_s, e_r, z_s, z_r)
    scale = row_scale(sq_bufs[1])
    owned = reduce_end(0, a, r1, r2, z_s, z_r)
    queries = silu(owned[0] * scale)
    forget_raw = owned[1] * scale
    fresh = owned[2] * scale
    gates = silu(owned[3] * scale)
    nseq = RL // W
    row = lax.broadcasted_iota(jnp.int32, (RL, 1), 0)
    slot_len = jnp.zeros((RL, 1), jnp.int32)
    for s in range(nseq):
        slot_len = jnp.where(row // W == s, lengths[k * nseq + s], slot_len)
    live = (row % W) < slot_len
    fl = floor[...]
    forgets = jnp.where(live, fl + (1.0 - fl) * sigmoid(forget_raw), 1.0)
    later["st"].wait()
    for h in range(HL // DK):
        hs = slice(h * DK, (h + 1) * DK)
        f_t = forgets[:, hs].T
        q_t = queries[:, hs].T
        for s in range(nseq):
            carried = st[s, h]
            for o in range(W):
                r = s * W + o
                f_col = jnp.broadcast_to(f_t[:, r:r + 1], (DK, DK))
                carried = f_col * carried + (1.0 - f_col) * fresh[r:r + 1, hs]
                ro[r:r + 1, hs] = jnp.sum(q_t[:, r:r + 1] * carried, axis=0, keepdims=True)
            st[s, h] = carried
    st_out = load(st, ns_h, st_sem.at[1])
    live32 = live.astype(F32)
    hg, hg_s, hg_r = hg_bufs
    for h in range(HL // DK):
        hs = slice(h * DK, (h + 1) * DK)
        read = ro[:, hs]
        meansq = jnp.mean(read * read, axis=1, keepdims=True)
        hg[k, :, hs] = (read * lax.rsqrt(meansq + EPSILON) * head_gain[...] * gates[:, hs] * live32).astype(BF16)
    for d in range(1, NK):
        send(hg.at[k], hg.at[k], hg_s.at[d - 1], hg_r.at[d - 1], ((k + d) % NK, t))
    later["mw"].wait()
    for d in range(1, NK):
        arrived(hg.at[(k - d + NK) % NK], hg_s.at[d - 1], hg_r.at[d - 1])
    heads = hg[...].astype(F32).reshape(ROWS, HL).astype(BF16)
    total = sum_tp(jnp.dot(heads, wmw[...], preferred_element_type=F32), ar_bufs[1])
    x2[...] = (x1[...].astype(F32) + total).astype(BF16)

    part = block(x2[...].astype(F32), g_post, wsg, wsu, wsd, later["sgu"], later["sd"], lambda: None,
                 sq_bufs[2], ffn_bufs[1])
    buf, ss, rs = ar_bufs[2]
    if aligned:
        p_send, p_own = fin
        p_own[...] = part
        p_send[...] = part.astype(BF16)
        for d in range(1, NT):
            peer = (t + d) % NT
            send(p_send.at[:, pl.ds(pl.multiple_of(peer * w_tok, w_tok), w_tok)], buf.at[d - 1],
                 ss.at[d - 1], rs.at[d - 1], (k, peer))
        total = p_own[:, mine]
        for d in range(1, NT):
            arrived(buf.at[d - 1], ss.at[d - 1], rs.at[d - 1])
            total = total + buf[d - 1].astype(F32)
        out[...] = (x2[:, mine].astype(F32) + 0.5 * total).astype(BF16)
    else:
        total = sum_tp(part, ar_bufs[2])
        out[...] = (x2[...].astype(F32) + 0.5 * total).astype(BF16)
    for cp in pending:
        cp.wait_send()
    st_out.wait()


def local(NK, NT, tokens, lengths, states, gain_pre, pre_gate, pre_up, pre_down, gain_mix, query_weight,
          forget_weight, input_weight, outgate_weight, forget_floor, head_gain, mix_weight, gain_post, post_gate,
          post_up, post_down):
    ROWS, w_tok = tokens.shape
    C, FL = pre_gate.shape
    HL = query_weight.shape[1]
    NZ = NK // CORES
    RL = ROWS // NK
    aligned = w_tok % 128 == 0
    nch = 2 if FL % 256 == 0 else 1
    FC = FL // nch
    if not aligned:
        tokens = lax.all_gather(tokens, "tp", axis=1, tiled=True)
    vm = lambda shape, dt=BF16: pltpu.VMEM(shape, dt)
    sem = lambda *shape: pltpu.SemaphoreType.DMA(shape)
    scratch = [vm((ROWS, C))] * 3 + [
        vm((C, FL)), vm((C, FL)), vm((FL, C)), vm((4, C, HL)), vm((HL, C)), vm((C, FL)), vm((C, FL)), vm((FL, C)),
        vm(states.shape, F32), sem(NT - 1), sem(NT - 1), sem(6 * nch + 5), sem(2)]
    for _ in range(3):
        scratch += [vm((NK, RL, 128), F32), vm((NK - 1, RL, 128), F32), sem(NK - 1), sem(NK - 1)]
    for _ in range(2):
        scratch += [
            vm((nch, 2, NZ, CORES, RL, FC), F32), vm((nch, 2, NZ, RL, FC)), vm((nch, 2, NZ, RL, FC)),
            vm((nch, NZ - 1, 2, RL, FC)), vm((nch, NZ - 1, 2, RL, FC)), vm((nch, NZ, CORES, RL, FC)),
            sem(nch), sem(nch), sem(nch, NZ - 1), sem(nch, NZ - 1), sem(nch, NZ - 1), sem(nch, NZ - 1),
            sem(nch, NZ), sem(nch, NZ)]
    scratch += [
        vm((1, 4, NZ, CORES, RL, HL), F32), vm((1, 4, NZ, RL, HL)), vm((1, 4, NZ, RL, HL)),
        vm((1, NZ - 1, 4, RL, HL)), vm((1, NZ - 1, 4, RL, HL)),
        sem(1), sem(1), sem(1, NZ - 1), sem(1, NZ - 1)]
    scratch += [vm((NK, RL, HL)), sem(NK - 1), sem(NK - 1), vm((RL, HL), F32)]
    for _ in range(2):
        scratch += [vm((NT, ROWS, C)), sem(NT - 1), sem(NT - 1)]
    scratch += [vm((NT - 1, ROWS, w_tok)) if aligned else vm((NT, ROWS, C)), sem(NT - 1), sem(NT - 1)]
    scratch += [vm((ROWS, C)), vm((ROWS, C), F32)]
    V = pl.BlockSpec(memory_space=pltpu.VMEM)
    A = pl.BlockSpec(memory_space=pl.ANY)
    S = pl.BlockSpec(memory_space=pltpu.SMEM)
    ow = w_tok if aligned else C
    finished, new_states = pl.pallas_call(
        functools.partial(kernel, (NK, NT, C, FL, HL, ROWS, aligned, nch)),
        out_shape=(jax.ShapeDtypeStruct((ROWS, ow), BF16), jax.ShapeDtypeStruct(states.shape, F32)),
        in_specs=[V, S, A, V, A, A, A, V, A, A, A, A, V, V, A, V, A, A, A],
        out_specs=(V, A),
        scratch_shapes=scratch,
        compiler_params=pltpu.CompilerParams(
            collective_id=0, has_side_effects=True, vmem_limit_bytes=60 * 1024 * 1024),
    )(tokens, lengths, states, gain_pre[None], pre_gate, pre_up, pre_down, gain_mix[None], query_weight,
      forget_weight, input_weight, outgate_weight, forget_floor[None], head_gain[None], mix_weight, gain_post[None],
      post_gate, post_up, post_down)
    if not aligned:
        finished = lax.dynamic_slice_in_dim(finished, lax.axis_index("tp") * w_tok, w_tok, axis=1)
    live_rows = (jnp.arange(W, dtype=jnp.int32)[None, :] < lengths[:, None]).reshape(-1, 1)
    return jnp.where(live_rows, finished, jnp.zeros_like(finished)), new_states


def solution(mesh):
    placed = (
        P(None, ("kv", "tp")), P(), P("kv", "tp", None, None),
        P("kv"), P("kv", "tp"), P("kv", "tp"), P("tp", "kv"),
        P("kv"), P("kv", "tp"), P("kv", "tp"), P("kv", "tp"), P("kv", "tp"), P("tp"), P(), P("tp", "kv"),
        P("kv"), P("kv", "tp"), P("kv", "tp"), P("tp", "kv"),
    )
    return jax.shard_map(
        functools.partial(local, mesh.shape["kv"], mesh.shape["tp"]),
        mesh=mesh,
        in_specs=placed,
        out_specs=(P(None, ("kv", "tp")), P("kv", "tp", None, None)),
        check_vma=False,
    )
```

time: 320 us -> 76.8 us (0.24)
  waiting for transfers between devices: 158 us -> 0 us
  blocking collectives: 112 us -> 0 us
  Pallas kernels: 0 us -> 71.8 us
  matrix products: 21.5 us -> 0 us
  between operations: 14.3 us -> 0.64 us
  other arithmetic: 11.7 us -> 2.13 us
    reduce_scatter x6 -> x0, waiting for transfers between devices: 158 us -> none  [the longest x2 62.5 us: half_mixer(): lax.psum_scatter(jnp.concatenate([jnp.dot(normed, gate_weight, preferred_...]
    pallas_call x0 -> x1, Pallas kernels: none -> 71.8 us  [local(): pl.pallas_call(functools.partial(kernel, (NK, NT, C, FL, HL, ROWS, aligne...]
    all_gather x6 -> x0, blocking collectives: 69.1 us -> none  [the longest x2 28.7 us: half_mixer(): lax.all_gather(hidden, 'kv', axis=0, tiled=True)]
    psum x3 -> x0, blocking collectives: 42.6 us -> none  [gathered_norm(): totals = lax.psum(block_squares, 'kv')]
    dot_general x15 -> x0, matrix products: 21.5 us -> none  [the longest x2 6.15 us: half_mixer(): jnp.dot(lax.all_gather(hidden, 'kv', axis=0, tiled=True), down_weight, pr...]
    convert_element_type x8 -> x0, other arithmetic: 5.85 us -> none  [the longest x2 1.94 us: half_mixer(): (jax.nn.silu(owned[:, :half_cols]) * owned[:, half_cols:]).astype(jnp.bfl...]
    concatenate x3 -> x0, other arithmetic: 3.25 us -> none  [the longest x2 2.42 us: half_mixer(): jnp.concatenate([jnp.dot(normed, gate_weight, preferred_element_type=jnp....]
  transfers between devices with their start and end apart: 6 -> 0, of which waited for: 6 -> 0; matrix products, arithmetic and copies ran while one was open for 0% -> 0% of each run, Pallas kernels for 0% -> 0%
where the time goes in v1:
time: 76.8 us; the launch traced here: 76.5 us
  Pallas kernels  71.8 us (93%)
  other arithmetic  2.13 us (3%)
  local copies, waits for them, and re-layouts  1.97 us (3%)
    pallas_call x1, Pallas kernels, local(): pl.pallas_call(functools.partial(kernel, (NK, NT, C, FL, HL, ROWS, aligne...  71.8 us
    unnamed x1, local copies, waits for them, and re-layouts  1.87 us

profile of v1, /device:TPU:0, one launch (start us, length us, event | category | flops | bytes accessed | tf_op | source)
XLA Modules:
  0.0 76.5 jit_solution(10630622861468292413)
XLA Ops:
  0.6 0.7 iota_compare_fusion
  1.4 0.1 lt.23
  1.5 71.8 %shard_map.194 = (bf16[64,128]{1,0:T(8,128)(2,1)}, f32[2,4,128,128]{3,2,1,0:T(8,128)}) custom-call(bf16[64,128]{1,0:T(8,128)(2,1)} %refs_0_.1, s32[16]{0:T(128)} %refs_1_.1, f32[2,4,128,128]{3,2,1,0:T(8,128)} %refs_2_.1, f32[1,512]{1,0:T(1,128)} %bitcast.5, bf16[512,2816]{1,0:T(8,128)(2,1)} %refs_4_.1, bf16[512,2816]{1,0:T(8,128)(2,1)} %refs_5_.1, ...), custom_call_target="tpu_custom_call" | custom-call | tf_op jit(solution)/shard_map/pallas_call | solution.py:324
  73.2 1.4 %broadcast_select_fusion = bf16[64,128]{1,0:T(8,128)(2,1)} fusion(bf16[64,128]{1,0:T(8,128)(2,1)} %get-tuple-element.4, pred[64]{0:T(512)(128)(4,1)S(1)} %lt.23), kind=kLoop, calls=%fused_computation | loop fusion | flops 8192 | bytes 32832 | tf_op jit(solution)/shard_map/jit(_where)/select_n | solution.py:338
  74.6 1.9 %copy.22 = f32[2,4,128,128]{3,2,1,0:T(8,128)} copy(f32[2,4,128,128]{3,2,1,0:T(8,128)} %get-tuple-element.9) | data formatting | bytes 1048576

commit v2 on v1

--- a/solution.py
+++ b/solution.py
@@ -26,10 +26,11 @@
 
 
 def kernel(cfg, *refs):
-    NK, NT, C, FL, HL, ROWS, aligned, nch = cfg
+    NK, NT, C, FL, HL, ROWS, aligned, widths = cfg
     NZ = NK // CORES
     RL = ROWS // NK
-    FC = FL // nch
+    nch = len(widths)
+    starts = [sum(widths[:j]) for j in range(nch)]
     it = iter(refs)
     (tokens, lengths, states_h, g_pre, pg_h, pu_h, pd_h, g_mix, q_h, f_h, i_h, o_h, floor, head_gain, mw_h,
      g_post, sg_h, su_h, sd_h) = [next(it) for _ in range(19)]
@@ -37,7 +38,7 @@
     (x0, x1, x2, wpg, wpu, wpd, wq, wmw, wsg, wsu, wsd, st, tok_s, tok_r, w_sem, st_sem) = [
         next(it) for _ in range(16)]
     sq_bufs = [[next(it) for _ in range(4)] for _ in range(3)]
-    ffn_bufs = [[next(it) for _ in range(14)] for _ in range(2)]
+    ffn_bufs = [[[next(it) for _ in range(14)] for _ in range(nch)] for _ in range(2)]
     mix_bufs = [next(it) for _ in range(9)]
     hg_bufs = [next(it) for _ in range(3)]
     ro = next(it)
@@ -69,7 +70,7 @@
         return cp
 
     def cols(j):
-        return pl.ds(j * FC, FC)
+        return pl.ds(starts[j], widths[j])
 
     sem_n = iter(range(64))
     pre_loads = []
@@ -115,59 +116,84 @@
 
     z_order = sorted(range(1, NZ), key=lambda d: -min(d, NZ - d))
 
-    def reduce_start(j, a, s1, r1, e_s, e_r):
-        s1[j] = a[j, :, :, oc].astype(BF16)
-        send(s1.at[j], r1.at[j], e_s.at[j], e_r.at[j], partner)
-
-    def reduce_middle(j, a, r1, s2, r2, e_s, e_r, z_s, z_r):
-        arrived(r1.at[j], e_s.at[j], e_r.at[j])
+    def two_terms(v):
+        high = v.astype(BF16)
+        return jnp.concatenate([high, (v - high.astype(F32)).astype(BF16)], axis=0)
+
+    def two_term_dot(v, w):
+        both = jnp.dot(v, w, preferred_element_type=F32)
+        return both[:ROWS] + both[ROWS:]
+
+    def reduce_start(bufs):
+        a, s1, r1, s2, r2, e_s, e_r, z_s, z_r = bufs
+        s1[...] = a[:, :, oc]
+        send(s1, r1, e_s.at[0], e_r.at[0], partner)
+
+    def reduce_middle(bufs):
+        a, s1, r1, s2, r2, e_s, e_r, z_s, z_r = bufs
+        arrived(r1, e_s.at[0], e_r.at[0])
         for d in z_order:
             zp = (z + d) % NZ
-            s2[j, d - 1] = (a[j, :, zp, c] + r1[j, :, zp].astype(F32)).astype(BF16)
-            send(s2.at[j, d - 1], r2.at[j, d - 1], z_s.at[j, d - 1], z_r.at[j, d - 1], (zp * CORES + c, t))
-
-    def reduce_end(j, a, r1, r2, z_s, z_r):
-        total = a[j, :, z, c] + r1[j, :, z].astype(F32)
+            s2[d - 1] = (a[:, zp, c] + r1[:, zp]).astype(BF16)
+            send(s2.at[d - 1], r2.at[d - 1], z_s.at[d - 1], z_r.at[d - 1], (zp * CORES + c, t))
+
+    def reduce_end(bufs):
+        a, s1, r1, s2, r2, e_s, e_r, z_s, z_r = bufs
+        total = a[:, z, c] + r1[:, z]
         for d in range(1, NZ):
-            arrived(r2.at[j, d - 1], z_s.at[j, d - 1], z_r.at[j, d - 1])
-            total = total + r2[j, d - 1].astype(F32)
+            arrived(r2.at[d - 1], z_s.at[d - 1], z_r.at[d - 1])
+            total = total + r2[d - 1].astype(F32)
         return total
 
     def block(x32, gain, wg, wu, wd, gu_loads, d_loads, after, sq, bufs):
-        a, s1, r1, s2, r2, hid, e_s, e_r, z_s, z_r, h_s, h_r, p_s, p_r = bufs
         squares(x32, sq)
-        y = (x32 * gain[...]).astype(BF16)
+        y = two_terms(x32 * gain[...])
         for j in range(nch):
             for cp in gu_loads[j]:
                 cp.wait()
             if j == nch - 1:
                 after()
             for g, w in enumerate((wg, wu)):
-                prod = jnp.dot(y, w[:, cols(j)], preferred_element_type=F32)
-                a[j, g] = prod.reshape(NZ, CORES, RL, FC)
-            reduce_start(j, a, s1, r1, e_s, e_r)
+                prod = two_term_dot(y, w[:, cols(j)])
+                bufs[j][0][g] = prod.reshape(NZ, CORES, RL, widths[j])
+            reduce_start(bufs[j][:9])
+            if j:
+                reduce_middle(bufs[j - 1][:9])
+        reduce_middle(bufs[nch - 1][:9])
+        scale = row_scale(sq)
+
+        def forward(j):
+            hid, h_s, h_r, p_s, p_r = bufs[j][9:]
+            for d in reversed(z_order):
+                src = hid.at[(z - d + NZ) % NZ, c]
+                arrived(src, h_s.at[d - 1], h_r.at[d - 1])
+                send(src, src, p_s.at[d], p_r.at[d], partner)
+
+        def down(j):
+            hid, h_s, h_r, p_s, p_r = bufs[j][9:]
+            d_loads[j].wait()
+            for d in range(NZ):
+                arrived(hid.at[(z - d + NZ) % NZ, oc], p_s.at[d], p_r.at[d])
+            h = hid[...].astype(F32).reshape(ROWS, widths[j]).astype(BF16)
+            return jnp.dot(h, wd[cols(j), :], preferred_element_type=F32)
+
         for j in range(nch):
-            reduce_middle(j, a, r1, s2, r2, e_s, e_r, z_s, z_r)
-        scale = row_scale(sq)
-        for j in range(nch):
-            total = reduce_end(j, a, r1, r2, z_s, z_r)
-            hid[j, z, c] = (silu(total[0] * scale) * (total[1] * scale)).astype(BF16)
-            own = hid.at[j, z, c]
+            hid, h_s, h_r, p_s, p_r = bufs[j][9:]
+            total = reduce_end(bufs[j][:9])
+            hid[z, c] = (silu(total[0] * scale) * (total[1] * scale)).astype(BF16)
+            own = hid.at[z, c]
             for d in z_order:
-                send(own, own, h_s.at[j, d - 1], h_r.at[j, d - 1], (((z + d) % NZ) * CORES + c, t))
-            send(own, own, p_s.at[j, 0], p_r.at[j, 0], partner)
-        for j in range(nch):
-            for d in reversed(z_order):
-                src = hid.at[j, (z - d + NZ) % NZ, c]
-                arrived(src, h_s.at[j, d - 1], h_r.at[j, d - 1])
-                send(src, src, p_s.at[j, d], p_r.at[j, d], partner)
+                send(own, own, h_s.at[d - 1], h_r.at[d - 1], (((z + d) % NZ) * CORES + c, t))
+            send(own, own, p_s.at[0], p_r.at[0], partner)
+            if j >= 2:
+                forward(j - 2)
+        for j in range(max(nch - 2, 0), nch - 1):
+            forward(j)
         part = None
         for j in range(nch):
-            d_loads[j].wait()
-            for d in range(NZ):
-                arrived(hid.at[j, (z - d + NZ) % NZ, oc], p_s.at[j, d], p_r.at[j, d])
-            h = hid[j].astype(F32).reshape(ROWS, FC).astype(BF16)
-            term = jnp.dot(h, wd[pl.ds(j * FC, FC), :], preferred_element_type=F32)
+            if j == min(1, nch - 1):
+                forward(nch - 1)
+            term = down(j)
             part = term if part is None else part + term
         return part
 
@@ -186,7 +212,7 @@
     later = {}
 
     def start_later():
-        later["pd"] = [load(pd_h.at[pl.ds(j * FC, FC)], wpd.at[pl.ds(j * FC, FC)], w_sem.at[next(sem_n)])
+        later["pd"] = [load(pd_h.at[cols(j)], wpd.at[cols(j)], w_sem.at[next(sem_n)])
                        for j in range(nch)]
         later["q"] = [load(h, wq.at[n], w_sem.at[next(sem_n)]) for n, h in enumerate((q_h, f_h, i_h, o_h))]
         later["st"] = load(states_h, st, st_sem.at[0])
@@ -194,7 +220,7 @@
         later["sgu"] = [[load(sg_h.at[:, cols(j)], wsg.at[:, cols(j)], w_sem.at[next(sem_n)]),
                          load(su_h.at[:, cols(j)], wsu.at[:, cols(j)], w_sem.at[next(sem_n)])]
                         for j in range(nch)]
-        later["sd"] = [load(sd_h.at[pl.ds(j * FC, FC)], wsd.at[pl.ds(j * FC, FC)], w_sem.at[next(sem_n)])
+        later["sd"] = [load(sd_h.at[cols(j)], wsd.at[cols(j)], w_sem.at[next(sem_n)])
                        for j in range(nch)]
 
     class Lazy:
@@ -206,16 +232,15 @@
     x1[...] = (x0[...].astype(F32) + 0.5 * total).astype(BF16)
 
     x32 = x1[...].astype(F32)
-    a, s1, r1, s2, r2, e_s, e_r, z_s, z_r = mix_bufs
     squares(x32, sq_bufs[1])
-    y = (x32 * g_mix[...]).astype(BF16)
+    y = two_terms(x32 * g_mix[...])
     for g in range(4):
         later["q"][g].wait()
-        a[0, g] = jnp.dot(y, wq[g], preferred_element_type=F32).reshape(NZ, CORES, RL, HL)
-    reduce_start(0, a, s1, r1, e_s, e_r)
-    reduce_middle(0, a, r1, s2, r2, e_s, e_r, z_s, z_r)
+        mix_bufs[0][g] = two_term_dot(y, wq[g]).reshape(NZ, CORES, RL, HL)
+    reduce_start(mix_bufs)
+    reduce_middle(mix_bufs)
     scale = row_scale(sq_bufs[1])
-    owned = reduce_end(0, a, r1, r2, z_s, z_r)
+    owned = reduce_end(mix_bufs)
     queries = silu(owned[0] * scale)
     forget_raw = owned[1] * scale
     fresh = owned[2] * scale
@@ -260,6 +285,11 @@
 
     part = block(x2[...].astype(F32), g_post, wsg, wsu, wsd, later["sgu"], later["sd"], lambda: None,
                  sq_bufs[2], ffn_bufs[1])
+    row = lax.broadcasted_iota(jnp.int32, (ROWS, 1), 0)
+    row_len = jnp.zeros((ROWS, 1), jnp.int32)
+    for s in range(ROWS // W):
+        row_len = jnp.where(row // W == s, lengths[s], row_len)
+    live_rows = ((row % W) < row_len).astype(F32)
     buf, ss, rs = ar_bufs[2]
     if aligned:
         p_send, p_own = fin
@@ -273,10 +303,10 @@
         for d in range(1, NT):
             arrived(buf.at[d - 1], ss.at[d - 1], rs.at[d - 1])
             total = total + buf[d - 1].astype(F32)
-        out[...] = (x2[:, mine].astype(F32) + 0.5 * total).astype(BF16)
+        out[...] = ((x2[:, mine].astype(F32) + 0.5 * total) * live_rows).astype(BF16)
     else:
         total = sum_tp(part, ar_bufs[2])
-        out[...] = (x2[...].astype(F32) + 0.5 * total).astype(BF16)
+        out[...] = ((x2[...].astype(F32) + 0.5 * total) * live_rows).astype(BF16)
     for cp in pending:
         cp.wait_send()
     st_out.wait()
@@ -291,8 +321,11 @@
     NZ = NK // CORES
     RL = ROWS // NK
     aligned = w_tok % 128 == 0
-    nch = 2 if FL % 256 == 0 else 1
-    FC = FL // nch
+    tiles = FL // 256
+    pieces = min(2, tiles)
+    widths = (FL,) if FL % 256 else tuple(
+        256 * (tiles // pieces + (1 if j < tiles % pieces else 0)) for j in range(pieces))
+    nch = len(widths)
     if not aligned:
         tokens = lax.all_gather(tokens, "tp", axis=1, tiled=True)
     vm = lambda shape, dt=BF16: pltpu.VMEM(shape, dt)
@@ -302,16 +335,18 @@
         vm(states.shape, F32), sem(NT - 1), sem(NT - 1), sem(6 * nch + 5), sem(2)]
     for _ in range(3):
         scratch += [vm((NK, RL, 128), F32), vm((NK - 1, RL, 128), F32), sem(NK - 1), sem(NK - 1)]
+
+    def reduce_bufs(parts, width):
+        return [
+            vm((parts, NZ, CORES, RL, width), F32), vm((parts, NZ, RL, width), F32), vm((parts, NZ, RL, width), F32),
+            vm((NZ - 1, parts, RL, width)), vm((NZ - 1, parts, RL, width)),
+            sem(1), sem(1), sem(NZ - 1), sem(NZ - 1)]
+
     for _ in range(2):
-        scratch += [
-            vm((nch, 2, NZ, CORES, RL, FC), F32), vm((nch, 2, NZ, RL, FC)), vm((nch, 2, NZ, RL, FC)),
-            vm((nch, NZ - 1, 2, RL, FC)), vm((nch, NZ - 1, 2, RL, FC)), vm((nch, NZ, CORES, RL, FC)),
-            sem(nch), sem(nch), sem(nch, NZ - 1), sem(nch, NZ - 1), sem(nch, NZ - 1), sem(nch, NZ - 1),
-            sem(nch, NZ), sem(nch, NZ)]
-    scratch += [
-        vm((1, 4, NZ, CORES, RL, HL), F32), vm((1, 4, NZ, RL, HL)), vm((1, 4, NZ, RL, HL)),
-        vm((1, NZ - 1, 4, RL, HL)), vm((1, NZ - 1, 4, RL, HL)),
-        sem(1), sem(1), sem(1, NZ - 1), sem(1, NZ - 1)]
+        for width in widths:
+            scratch += reduce_bufs(2, width) + [
+                vm((NZ, CORES, RL, width)), sem(NZ - 1), sem(NZ - 1), sem(NZ), sem(NZ)]
+    scratch += reduce_bufs(4, HL)
     scratch += [vm((NK, RL, HL)), sem(NK - 1), sem(NK - 1), vm((RL, HL), F32)]
     for _ in range(2):
         scratch += [vm((NT, ROWS, C)), sem(NT - 1), sem(NT - 1)]
@@ -322,7 +357,7 @@
     S = pl.BlockSpec(memory_space=pltpu.SMEM)
     ow = w_tok if aligned else C
     finished, new_states = pl.pallas_call(
-        functools.partial(kernel, (NK, NT, C, FL, HL, ROWS, aligned, nch)),
+        functools.partial(kernel, (NK, NT, C, FL, HL, ROWS, aligned, widths)),
         out_shape=(jax.ShapeDtypeStruct((ROWS, ow), BF16), jax.ShapeDtypeStruct(states.shape, F32)),
         in_specs=[V, S, A, V, A, A, A, V, A, A, A, A, V, V, A, V, A, A, A],
         out_specs=(V, A),
@@ -334,8 +369,7 @@
       post_gate, post_up, post_down)
     if not aligned:
         finished = lax.dynamic_slice_in_dim(finished, lax.axis_index("tp") * w_tok, w_tok, axis=1)
-    live_rows = (jnp.arange(W, dtype=jnp.int32)[None, :] < lengths[:, None]).reshape(-1, 1)
-    return jnp.where(live_rows, finished, jnp.zeros_like(finished)), new_states
+    return finished, new_states
 
 
 def solution(mesh):

time: 76.8 us -> 77.1 us (level)
  other arithmetic: 2.13 us -> 0 us
  local copies, waits for them, and re-layouts: 1.97 us -> 3.2 us
  Pallas kernels: 71.8 us -> 73 us
    select_n x1 -> x0, other arithmetic: 1.4 us -> none  [local(): jnp.where(live_rows, finished, jnp.zeros_like(finished))]
    unnamed x1 -> x2, local copies, waits for them, and re-layouts: 1.87 us -> 3.2 us
    pallas_call x1, Pallas kernels: 71.8 us -> 73 us  [local(): pl.pallas_call(functools.partial(kernel, (NK, NT, C, FL, HL, ROWS, aligne...]
where the time goes in v2:
time: 77.1 us; the launch traced here: 76.9 us
  Pallas kernels  73 us (95%)
  local copies, waits for them, and re-layouts  3.2 us (4%)
    pallas_call x1, Pallas kernels, local(): pl.pallas_call(functools.partial(kernel, (NK, NT, C, FL, HL, ROWS, aligne...  73 us
    unnamed x2, local copies, waits for them, and re-layouts  3.2 us

profile of v2, /device:TPU:0, one launch (start us, length us, event | category | flops | bytes accessed | tf_op | source)
XLA Modules:
  0.0 76.9 jit_solution(6549664381040023280)
XLA Ops:
  0.6 73.0 %shard_map.194 = (bf16[64,128]{1,0:T(8,128)(2,1)}, f32[2,4,128,128]{3,2,1,0:T(8,128)}) custom-call(bf16[64,128]{1,0:T(8,128)(2,1)} %refs_0_.1, s32[16]{0:T(128)} %refs_1_.1, f32[2,4,128,128]{3,2,1,0:T(8,128)} %refs_2_.1, f32[1,512]{1,0:T(1,128)} %bitcast.5, bf16[512,2816]{1,0:T(8,128)(2,1)} %refs_4_.1, bf16[512,2816]{1,0:T(8,128)(2,1)} %refs_5_.1, ...), custom_call_target="tpu_custom_call" | custom-call | tf_op jit(solution)/shard_map/pallas_call | solution.py:359
  73.7 1.3 %copy.23 = bf16[64,128]{1,0:T(8,128)(2,1)} copy(bf16[64,128]{1,0:T(8,128)(2,1)} %get-tuple-element.4) | data formatting | bytes 32768
  75.0 1.9 %copy.24 = f32[2,4,128,128]{3,2,1,0:T(8,128)} copy(f32[2,4,128,128]{3,2,1,0:T(8,128)} %get-tuple-element.5) | data formatting | bytes 1048576
